TPU v7x, 32 devices: a whole 2x2x4 slice. The times are simulated.
32 devices in a mesh: rep: 2 (over x), fs: 4 (over z), tp: 4 (over y, core).
Axes of the slice: x: 2, y: 2, z: 4, core: 2. Of those that a mesh axis runs over, the one named last changes fastest.
Arguments:
- tokens: bfloat16 [3072, 2048], P(('rep', 'fs'), 'tp'), may hold values from -6 to 6
- norm_gain: bfloat16 [2048], replicated, may hold values from 0.099609375 to 1.8984375
- w_gate: bfloat16 [2048, 5120], P('fs', 'tp'), may hold values from -0.125 to 0.125
- w_up: bfloat16 [2048, 5120], P('fs', 'tp'), may hold values from -0.125 to 0.125
- w_down: bfloat16 [5120, 2048], P('tp', 'fs'), may hold values from -0.078125 to 0.078125
- cotangent: bfloat16 [3072, 2048], P(('rep', 'fs'), 'tp'), may hold values from -6 to 6
Outputs:
- grad_tokens: bfloat16 [3072, 2048], P(('rep', 'fs'), 'tp')
- grad_gain: float32 [2048], P('tp')
- grad_gate: float32 [2048, 5120], P('fs', 'tp')
- grad_up: float32 [2048, 5120], P('fs', 'tp')
- grad_down: float32 [5120, 2048], P('tp', 'fs')
- gate_up_sq: float32 [2, 2048], P(None, 'fs')
- down_sq: float32 [5120], P('tp')
All inputs are finite; a program needn't handle non-finite values.
Results may differ from a plain program's by a relative error of at most 0.018.
Values may be sent and summed in bfloat16 or wider, within the bound.
A program may use at most 128 MiB of HBM per device.

v0:
```python
import jax
import jax.numpy as jnp
from jax import lax
from jax.sharding import PartitionSpec as P


def contract_last(left, right):
    return lax.dot_general(
        left, right, (((1,), (1,)), ((), ())), preferred_element_type=jnp.float32
    )


def on_device(tokens, norm_gain, w_gate, w_up, w_down, cotangent):
    whole_x, whole_dy = (
        lax.all_gather(tokens, "tp", axis=1, tiled=True),
        lax.all_gather(cotangent, "tp", axis=1, tiled=True),
    )
    width = whole_x.shape[1]
    wide_tokens = whole_x.astype(jnp.float32)
    gain_f = norm_gain.astype(jnp.float32)
    inverse = lax.rsqrt(jnp.mean(wide_tokens * wide_tokens, axis=-1, keepdims=True) + 1e-06)
    normed = (wide_tokens * inverse * gain_f).astype(jnp.bfloat16)
    hidden_local = w_gate.shape[1]
    pieces = (
        lax.all_gather(w_gate, "fs", axis=0, tiled=True),
        lax.all_gather(w_up, "fs", axis=0, tiled=True),
    )
    columns = normed
    gate = jnp.dot(columns, pieces[0], preferred_element_type=jnp.float32)
    up_proj = jnp.dot(columns, pieces[1], preferred_element_type=jnp.float32)
    columns = whole_dy
    back = 0.5 * contract_last(columns, lax.all_gather(w_down, "fs", axis=1, tiled=True))
    sigma = jax.nn.sigmoid(gate)
    active = gate * sigma
    hidden = (active * up_proj).astype(jnp.bfloat16)
    d_up = (back * active).astype(jnp.bfloat16)
    d_gate = (back * up_proj * sigma * (1.0 + gate * (1.0 - sigma))).astype(jnp.bfloat16)
    pieces = lax.all_gather((w_gate, w_up), "fs", axis=0, tiled=True)
    partial_normed = contract_last(d_gate, pieces[0]) + contract_last(d_up, pieces[1])
    d_normed = lax.psum_scatter(
        partial_normed.astype(jnp.bfloat16), "tp", scatter_dimension=1, tiled=True
    ).astype(jnp.float32)
    local_width = d_normed.shape[1]
    local_gain = lax.dynamic_slice_in_dim(
        gain_f, lax.axis_index("tp") * local_width, local_width, 0
    )
    local_tokens = tokens.astype(jnp.float32)
    scaled_grad = d_normed * local_gain
    rowdot = lax.psum(jnp.sum(scaled_grad * local_tokens, axis=-1), "tp")
    grad_tokens = (
        cotangent.astype(jnp.float32)
        + inverse * scaled_grad
        - local_tokens * inverse**3 * rowdot[:, None] / width
    ).astype(jnp.bfloat16)
    grad_gain = lax.psum(jnp.sum(d_normed * local_tokens * inverse, axis=0), ("rep", "fs"))
    paired = jnp.concatenate([d_gate, d_up], axis=1)
    fs_count = lax.axis_size("fs")
    rep_count = lax.axis_size("rep")
    first = jnp.einsum("td,tf->df", normed, paired, preferred_element_type=jnp.float32)
    second = 0.5 * jnp.einsum("td,tf->df", whole_dy, hidden, preferred_element_type=jnp.float32)
    full_term = jnp.concatenate([first, second], axis=1)
    each_rows = width // (rep_count * fs_count)
    reordered = jnp.swapaxes(
        full_term.reshape(fs_count, rep_count, each_rows, full_term.shape[1]), 0, 1
    )
    reordered = reordered.reshape(width, full_term.shape[1])
    summed = lax.psum_scatter(
        reordered.astype(jnp.bfloat16), ("rep", "fs"), scatter_dimension=0, tiled=True
    ).astype(jnp.float32)
    owned = lax.all_gather(summed.astype(jnp.bfloat16), "rep", axis=0, tiled=True).astype(
        summed.dtype
    )
    grad_gate = owned[:, :hidden_local]
    grad_up = owned[:, hidden_local : 2 * hidden_local]
    down_part = owned[:, 2 * hidden_local :]
    grad_down = down_part.T
    gate_up_sq = lax.psum(
        jnp.stack([jnp.sum(grad_gate * grad_gate, axis=1), jnp.sum(grad_up * grad_up, axis=1)]),
        "tp",
    )
    down_sq = lax.psum(jnp.sum(down_part * down_part, axis=0), "fs")
    return (grad_tokens, grad_gain, grad_gate, grad_up, grad_down, gate_up_sq, down_sq)


def solution(mesh):
    placed = (
        P(("rep", "fs"), "tp"),
        P(),
        P("fs", "tp"),
        P("fs", "tp"),
        P("tp", "fs"),
        P(("rep", "fs"), "tp"),
    )
    return jax.shard_map(
        on_device,
        mesh=mesh,
        in_specs=placed,
        out_specs=(
            P(("rep", "fs"), "tp"),
            P("tp"),
            P("fs", "tp"),
            P("fs", "tp"),
            P("tp", "fs"),
            P(None, "fs"),
            P("tp"),
        ),
        check_vma=False,
    )
```

profile of v0, /device:TPU:0, one launch (start us, length us, event | category | flops | bytes accessed | tf_op | source)
XLA Modules:
  0.0 797.0 jit_solution(14903006914669137343)
XLA Ops:
  8.0 0.7 all-gather.15.cloned.1.call-update
  8.7 0.7 all-gather.13.cloned.1.call-update
  10.6 21.3 %all-gather.7.cloned.1.call-done = bf16[384,2048]{1,0:T(8,128)(2,1)} async-done(((bf16[384,512]{1,0:T(8,128)(2,1)}), bf16[384,2048]{1,0:T(8,128)(2,1)}) %all-gather.7.cloned.1.call-update) | async-done | bytes 1572880 | tf_op jit(solution)/shard_map/all_gather | solution.py:15
  31.9 1.8 fusion.1
  33.7 97.8 %all-gather.15.cloned.1.call-done = bf16[2048,1280]{1,0:T(8,128)(2,1)} async-done(((bf16[512,1280]{1,0:T(8,128)(2,1)}), bf16[2048,1280]{1,0:T(8,128)(2,1)}) %all-gather.15.cloned.1.call-update) | async-done | bytes 5242896 | tf_op jit(solution)/shard_map/all_gather | solution.py:25
  131.6 6.6 fusion.21
  138.2 91.4 %all-gather.13.cloned.1.call-done = bf16[2048,1280]{1,0:T(8,128)(2,1)} async-done(((bf16[512,1280]{1,0:T(8,128)(2,1)}), bf16[2048,1280]{1,0:T(8,128)(2,1)}) %all-gather.13.cloned.1.call-update) | async-done | bytes 5242896 | tf_op jit(solution)/shard_map/all_gather | solution.py:26
  229.6 6.0 fusion.23
  235.6 13.4 %all-gather.9.cloned.1.call-done = bf16[384,2048]{1,0:T(8,128)(2,1)} async-done(((bf16[384,512]{1,0:T(8,128)(2,1)}), bf16[384,2048]{1,0:T(8,128)(2,1)}) %all-gather.9.cloned.1.call-update) | async-done | bytes 1572880 | tf_op jit(solution)/shard_map/all_gather | solution.py:16
  249.0 7.9 fusion
  256.9 91.5 %all-gather.11.cloned.1.call-done = bf16[1280,2048]{1,0:T(8,128)(2,1)} async-done(((bf16[1280,512]{1,0:T(8,128)(2,1)}), bf16[1280,2048]{1,0:T(8,128)(2,1)}) %all-gather.11.cloned.1.call-update) | async-done | bytes 5242896 | tf_op jit(solution)/shard_map/all_gather | solution.py:32
  348.5 6.9 multiply_convert_fusion.2
  355.4 6.4 convolution_convert_fusion
  361.8 6.4 pad_maximum_fusion
  368.2 26.2 %copy.14 = bf16[2,4,256,3840]{2,1,0,3:T(4,128)(2,1)} copy(bf16[2,4,256,3840]{3,2,0,1:T(8,128)(2,1)} %bitcast.20) | data formatting | bytes 31457280 | tf_op jit(solution)/shard_map/convert_element_type | solution.py:68
  394.4 25.9 %convert_element_type.61 = bf16[2048,3840]{0,1:T(8,128)(2,1)} reshape(bf16[2,4,256,3840]{2,1,0,3:T(4,128)(2,1)} %copy.14) | data formatting | bytes 31457280 | tf_op jit(solution)/shard_map/convert_element_type | solution.py:68
  420.3 1.1 copy-done.7
  421.5 4.7 fusion.26
  426.2 6.3 add_convert_fusion
  432.6 237.9 %reduce-scatter.5.cloned.1.call-done = bf16[256,3840]{0,1:T(8,128)(2,1)} async-done(((bf16[2048,3840]{0,1:T(8,128)(2,1)}), bf16[256,3840]{0,1:T(8,128)(2,1)}) %reduce-scatter.5.cloned.1.call-update) | async-done | bytes 1966096 | tf_op jit(solution)/shard_map/reduce_scatter | solution.py:67
  670.6 30.1 %reduce-scatter.3.cloned.1.call-done = bf16[384,512]{1,0:T(8,128)(2,1)} async-done(((bf16[384,2048]{1,0:T(8,128)(2,1)}), bf16[384,512]{1,0:T(8,128)(2,1)}) %reduce-scatter.3.cloned.1.call-update) | async-done | bytes 393232 | tf_op jit(solution)/shard_map/reduce_scatter | solution.py:40
  700.7 1.3 fusion.16
  702.1 22.4 %psum.29 = f32[512]{0:T(512)} all-reduce(f32[512]{0:T(512)S(1)} %get-tuple-element.17), channel_id=1, replica_groups=mesh['rep'=2,'fs'=4,'tp'=4] {'rep','fs'}, use_global_device_ids=true, to_apply=%region_5.0 | all-reduce | flops 512 | bytes 4096 | tf_op jit(solution)/shard_map/psum | solution.py:55
  724.4 31.8 %all-gather.17.cloned.1.call-done = bf16[512,3840]{0,1:T(8,128)(2,1)} async-done(((bf16[256,3840]{0,1:T(8,128)(2,1)}), bf16[512,3840]{0,1:T(8,128)(2,1)}) %all-gather.17.cloned.1.call-update) | async-done | bytes 3932176 | tf_op jit(solution)/shard_map/all_gather | solution.py:70
  756.2 3.9 fusion.25
  760.2 3.2 copy.16
  763.4 2.1 copy.15
  765.5 3.2 convert_element_type.62
  768.7 1.7 multiply_reduce_fusion
  770.5 12.3 %psum.31 = f32[1280]{0:T(1024)} all-reduce(f32[1280]{0:T(1024)S(1)} %get-tuple-element.14), channel_id=1, replica_groups=mesh['rep'=2,'fs'=4,'tp'=4] {'fs'}, use_global_device_ids=true, to_apply=%region_11.0 | all-reduce | flops 1280 | bytes 10240 | tf_op jit(solution)/shard_map/psum | solution.py:81
  782.8 6.3 all-reduce
  789.1 1.1 fusion.11
  (33 shorter events, 2.2 us)
Async XLA Ops:
  7.2 3.4 copy-start.5
  7.2 24.8 %all-gather.7.cloned.1.call-start = ((), (), s32[]{:S(2)}) async-start(), calls=%async_computation.2 | async-start | bytes 1966080 | tf_op jit(solution)/shard_map/all_gather | solution.py:15
  7.9 123.7 %all-gather.15.cloned.1.call-start = ((), (), s32[]{:S(2)}) async-start(), calls=%async_computation.6 | async-start | bytes 6553600 | tf_op jit(solution)/shard_map/all_gather | solution.py:25
  8.7 220.9 %all-gather.13.cloned.1.call-start = ((), (), s32[]{:S(2)}) async-start(), calls=%async_computation.5 | async-start | bytes 6553600 | tf_op jit(solution)/shard_map/all_gather | solution.py:26
  9.4 239.6 %all-gather.9.cloned.1.call-start = ((), (), s32[]{:S(2)}) async-start(), calls=%async_computation.3 | async-start | bytes 1966080 | tf_op jit(solution)/shard_map/all_gather | solution.py:16
  10.0 338.5 %all-gather.11.cloned.1.call-start = ((), (), s32[]{:S(2)}) async-start(), calls=%async_computation.4 | async-start | bytes 6553600 | tf_op jit(solution)/shard_map/all_gather | solution.py:32
  10.6 660.0 %reduce-scatter.5.cloned.1.call-start = ((), (), s32[]{:S(2)}) async-start(), calls=%async_computation.8 | async-start | bytes 17694720 | tf_op jit(solution)/shard_map/reduce_scatter | solution.py:67
  131.6 98.0 %copy-start.2 = (bf16[384,2048]{1,0:T(8,128)(2,1)S(1)}, bf16[384,2048]{1,0:T(8,128)(2,1)}, u32[]{:S(2)}) copy-start(bf16[384,2048]{1,0:T(8,128)(2,1)} %all-gather.7.cloned.1.call-done) | copy-start | bytes 4718596
  355.3 6.4 copy-start.6
  355.3 6.4 copy-start
  420.3 1.2 copy-start.7
  420.3 280.4 %reduce-scatter.3.cloned.1.call-start = ((), (), s32[]{:S(2)}) async-start(), calls=%async_computation.7 | async-start | bytes 1966080 | tf_op jit(solution)/shard_map/reduce_scatter | solution.py:40
  432.5 268.2 %copy-start.1 = (bf16[384,512]{1,0:T(8,128)(2,1)S(1)}, bf16[384,512]{1,0:T(8,128)(2,1)}, u32[]{:S(2)}) copy-start(bf16[384,512]{1,0:T(8,128)(2,1)} %param.6) | copy-start | bytes 1179652
  432.5 323.7 %all-gather.17.cloned.1.call-start = ((), (), s32[]{:S(2)}) async-start(), calls=%async_computation.9 | async-start | bytes 5898240 | tf_op jit(solution)/shard_map/all_gather | solution.py:70
  768.7 20.4 %copy-start.3 = (bf16[384,512]{1,0:T(8,128)(2,1)S(1)}, bf16[384,512]{1,0:T(8,128)(2,1)}, u32[]{:S(2)}) copy-start(bf16[384,512]{1,0:T(8,128)(2,1)} %param.11) | copy-start | bytes 1179652
  768.7 20.4 %copy-start.4 = (bf16[384,512]{1,0:T(8,128)(2,1)S(1)}, bf16[384,512]{1,0:T(8,128)(2,1)}, u32[]{:S(2)}) copy-start(bf16[384,512]{1,0:T(8,128)(2,1)} %reduce-scatter.3.cloned.1.call-done) | copy-start | bytes 1179652
Sparse Core Ops, SparseCore 0:
  9.5 22.3 all-gather.6
  33.5 98.0 all-gather.14
  133.1 96.3 all-gather.12
  231.0 17.9 all-gather.8
  250.4 98.0 all-gather.10
  420.4 250.0 reduce-scatter.4
  673.6 27.0 reduce-scatter.2
  702.3 53.9 all-gather.16
where the time goes:
time: 799 us; the launch traced here: 797 us
  waiting for transfers between devices  618 us (77%)
  local copies, waits for them, and re-layouts  62.5 us (8%)
  matrix products  44.9 us (6%)
  blocking collectives  41 us (5%)
  other arithmetic  15.6 us (2%)
  between operations  14.3 us (2%)
    reduce_scatter x1, waiting for transfers between devices, on_device(): lax.psum_scatter(reordered.astype(jnp.bfloat16), ('rep', 'fs'), scatter_d...  238 us
    all_gather x1, waiting for transfers between devices, on_device(): lax.all_gather(w_gate, 'fs', axis=0, tiled=True)  97.8 us
    all_gather x1, waiting for transfers between devices, on_device(): lax.all_gather(w_down, 'fs', axis=1, tiled=True)  91.5 us
    all_gather x1, waiting for transfers between devices, on_device(): lax.all_gather(w_up, 'fs', axis=0, tiled=True)  91.4 us
    convert_element_type x2, local copies, waits for them, and re-layouts, on_device(): reordered.astype(jnp.bfloat16)  52 us
    all_gather x1, waiting for transfers between devices, on_device(): lax.all_gather(summed.astype(jnp.bfloat16), 'rep', axis=0, tiled=True)  31.8 us
    reduce_scatter x1, waiting for transfers between devices, on_device(): lax.psum_scatter(partial_normed.astype(jnp.bfloat16), 'tp', scatter_dimen...  30.1 us
    psum x1, blocking collectives, on_device(): lax.psum(jnp.sum(d_normed * local_tokens * inverse, axis=0), ('rep', 'fs'))  22.4 us
  transfers between devices with their start and end apart: 8, of which 8 were waited for; matrix products, arithmetic and copies ran while one was open for 4% of the time, Pallas kernels for 0%

commit v1 on v0

v1 whole, which is shorter than its diff:
```python
import functools

import jax
import jax.numpy as jnp
from jax import lax
from jax.experimental import pallas as pl
from jax.experimental.pallas import tpu as pltpu
from jax.sharding import PartitionSpec as P

MESH = pl.DeviceIdType.MESH


def contract_last(left, right):
    return lax.dot_general(
        left, right, (((1,), (1,)), ((), ())), preferred_element_type=jnp.float32
    )


def contract_first(left, right):
    return lax.dot_general(
        left, right, (((0,), (0,)), ((), ())), preferred_element_type=jnp.float32
    )


def send(source, target, send_sem, recv_sem, where):
    copy = pltpu.make_async_remote_copy(
        src_ref=source,
        dst_ref=target,
        send_sem=send_sem,
        recv_sem=recv_sem,
        device_id=where,
        device_id_type=MESH,
    )
    copy.start()
    return copy


def greet(peers):
    barrier = pltpu.get_barrier_semaphore()
    for peer in peers:
        pl.semaphore_signal(barrier, inc=1, device_id=peer, device_id_type=MESH)
    pl.semaphore_wait(barrier, len(peers))


def keep_own(sources, holders, targets, sems):
    count = len(sources)
    loads = [
        pltpu.make_async_copy(sources[i], holders[i], sems.at[0, i]) for i in range(count)
    ]
    stores = [
        pltpu.make_async_copy(holders[i], targets[i], sems.at[1, i]) for i in range(count)
    ]
    for load in loads:
        load.start()

    def finish():
        for load, store in zip(loads, stores):
            load.wait()
            store.start()
        for store in stores:
            store.wait()

    return finish


def weights_kernel(n_fs, n_tp, *refs):
    tokens, cot, w_gate, w_up, w_down = refs[:5]
    whole_x, whole_dy, full_gate, full_up, full_down = refs[5:10]
    holders = refs[10:15]
    own_sem, ring_send, ring_recv, rep_send, rep_recv, tp_send, tp_recv = refs[15:]
    r, z, t = lax.axis_index("rep"), lax.axis_index("fs"), lax.axis_index("tp")
    right, left = lax.rem(z + 1, n_fs), lax.rem(z + n_fs - 1, n_fs)
    partner = {"rep": 1 - r}
    sources = (w_gate, w_up, w_down)
    targets = (full_gate, full_up, full_down)
    rows = w_gate.shape[0]
    hidden = w_down.shape[0]
    local = tokens.shape[1]
    reach = n_fs // 2

    def own_piece(m, half):
        size = (hidden if m == 2 else rows) // 2
        return sources[m].at[pl.ds(pl.multiple_of(half * size, size), size), :]

    def piece(m, owner, half):
        if m == 2:
            size = hidden // 2
            return targets[m].at[
                pl.ds(pl.multiple_of(half * size, size), size),
                pl.ds(pl.multiple_of(owner * rows, rows), rows),
            ]
        size = rows // 2
        return targets[m].at[
            pl.ds(pl.multiple_of(owner * rows + half * size, size), size), :
        ]

    peers = [{"fs": right}, {"fs": left}, partner]
    peers += [{"tp": lax.rem(t + j, n_tp)} for j in range(1, n_tp)]
    greet(peers)

    ends = []

    def hop(m, side, d):
        half = r if side == 0 else 1 - r
        owner = lax.rem(z + (n_fs - (d - 1) if side == 0 else d - 1), n_fs)
        place = piece(m, owner, half)
        return send(
            own_piece(m, half) if d == 1 else place,
            place,
            ring_send.at[m, side, d - 1],
            ring_recv.at[m, side, d - 1],
            {"fs": right if side == 0 else left},
        )

    flying = {}
    for m in range(3):
        for side in range(2):
            flying[m, side] = hop(m, side, 1)
    for a, (source, target) in enumerate(((tokens, whole_x), (cot, whole_dy))):
        place = target.at[:, pl.ds(pl.multiple_of(t * local, local), local)]
        for j in range(1, n_tp):
            ends.append(
                send(
                    source,
                    place,
                    tp_send.at[a, j - 1],
                    tp_recv.at[a, j - 1],
                    {"tp": lax.rem(t + j, n_tp)},
                )
            )
    mine = pl.ds(pl.multiple_of(t * local, local), local)
    band = pl.ds(pl.multiple_of(z * rows, rows), rows)
    finish = keep_own(
        (tokens, cot, w_gate, w_up, w_down),
        holders,
        (
            whole_x.at[:, mine],
            whole_dy.at[:, mine],
            full_gate.at[band, :],
            full_up.at[band, :],
            full_down.at[:, band],
        ),
        own_sem,
    )
    finish()
    for d in range(1, reach + 1):
        for m in range(3):
            for side in range(2):
                copy = flying[m, side]
                copy.wait_recv()
                if d < reach:
                    flying[m, side] = hop(m, side, d + 1)
                    half = r if side == 0 else 1 - r
                    owner = lax.rem(z + (n_fs - d if side == 0 else d), n_fs)
                    place = piece(m, owner, half)
                    ends.append(
                        send(
                            place,
                            place,
                            rep_send.at[m, side, d - 1],
                            rep_recv.at[m, side, d - 1],
                            partner,
                        )
                    )
                copy.wait_send()
    for copy in ends:
        copy.wait()


def gather_weights(n_fs, n_tp, tokens, cot, w_gate, w_up, w_down):
    count, local = tokens.shape
    rows, hidden = w_gate.shape
    width = rows * n_fs
    dtype = tokens.dtype
    shapes = [
        (count, width),
        (count, width),
        (width, hidden),
        (width, hidden),
        (hidden, width),
    ]
    held = (tokens, cot, w_gate, w_up, w_down)
    reach = n_fs // 2
    moved = sum(2 * a * b for a, b in shapes)
    dma = pltpu.SemaphoreType.DMA
    return pl.pallas_call(
        functools.partial(weights_kernel, n_fs, n_tp),
        out_shape=[jax.ShapeDtypeStruct(s, dtype) for s in shapes],
        in_specs=[pl.BlockSpec(memory_space=pl.ANY)] * 5,
        out_specs=[pl.BlockSpec(memory_space=pl.ANY)] * 5,
        scratch_shapes=[pltpu.VMEM(a.shape, a.dtype) for a in held]
        + [
            dma((2, 5)),
            dma((3, 2, reach)),
            dma((3, 2, reach)),
            dma((3, 2, max(reach - 1, 1))),
            dma((3, 2, max(reach - 1, 1))),
            dma((2, n_tp - 1)),
            dma((2, n_tp - 1)),
        ],
        compiler_params=pltpu.CompilerParams(collective_id=0, has_side_effects=True),
        cost_estimate=pl.CostEstimate(flops=0, bytes_accessed=16 * moved, transcendentals=0),
        name="gather_weights",
    )(*held)


def tokens_kernel(n_fs, n_act, n_swap, *refs):
    total = n_act + n_swap
    acts, swaps = refs[:n_act], refs[n_act:total]
    act_outs, swap_outs = refs[total : total + n_act], refs[total + n_act : 2 * total]
    holders = refs[2 * total : 3 * total]
    own_sem, ring_send, ring_recv, swap_send, swap_recv = refs[3 * total :]
    z = lax.axis_index("fs")
    right, left = lax.rem(z + 1, n_fs), lax.rem(z + n_fs - 1, n_fs)
    count = acts[0].shape[0]
    reach = n_fs // 2
    greet([{"fs": lax.rem(z + j, n_fs)} for j in range(1, n_fs)])

    def hop(m, side, d):
        owner = lax.rem(z + (n_fs - (d - 1) if side == 0 else d - 1), n_fs)
        first, size = 0, count
        if d == reach:
            size = count // 2
            first = side * size
        place = act_outs[m].at[pl.ds(pl.multiple_of(owner * count + first, size), size), :]
        source = acts[m].at[pl.ds(first, size), :] if d == 1 else place
        return send(
            source,
            place,
            ring_send.at[m, side, d - 1],
            ring_recv.at[m, side, d - 1],
            {"fs": right if side == 0 else left},
        )

    ends = []
    flying = {}
    band = pl.ds(pl.multiple_of(z * count, count), count)
    for m in range(n_act):
        for side in range(2):
            flying[m, side] = hop(m, side, 1)
    for a in range(n_swap):
        cut = swap_outs[a].shape[1]
        for j in range(1, n_fs):
            peer = lax.rem(z + j, n_fs)
            ends.append(
                send(
                    swaps[a].at[:, pl.ds(pl.multiple_of(peer * cut, cut), cut)],
                    swap_outs[a].at[band, :],
                    swap_send.at[a, j - 1],
                    swap_recv.at[a, j - 1],
                    {"fs": peer},
                )
            )
    sources = list(acts)
    for a in range(n_swap):
        cut = swap_outs[a].shape[1]
        sources.append(swaps[a].at[:, pl.ds(pl.multiple_of(z * cut, cut), cut)])
    finish = keep_own(
        sources, holders, [out.at[band, :] for out in act_outs + swap_outs], own_sem
    )
    finish()
    for d in range(1, reach + 1):
        for m in range(n_act):
            for side in range(2):
                copy = flying[m, side]
                copy.wait_recv()
                if d < reach:
                    flying[m, side] = hop(m, side, d + 1)
                copy.wait_send()
    for copy in ends:
        copy.wait()


def gather_tokens(n_fs, collective_id, acts, swaps):
    count = acts[0].shape[0]
    outs = [jax.ShapeDtypeStruct((n_fs * count, a.shape[1]), a.dtype) for a in acts]
    outs += [jax.ShapeDtypeStruct((n_fs * count, a.shape[1] // n_fs), a.dtype) for a in swaps]
    reach = n_fs // 2
    dma = pltpu.SemaphoreType.DMA
    total = len(outs)
    n_swap = max(len(swaps), 1)
    moved = sum(2 * o.shape[0] * o.shape[1] for o in outs)
    return pl.pallas_call(
        functools.partial(tokens_kernel, n_fs, len(acts), len(swaps)),
        out_shape=outs,
        in_specs=[pl.BlockSpec(memory_space=pl.ANY)] * total,
        out_specs=[pl.BlockSpec(memory_space=pl.ANY)] * total,
        scratch_shapes=[pltpu.VMEM((count, o.shape[1]), o.dtype) for o in outs]
        + [
            dma((2, total)),
            dma((len(acts), 2, reach)),
            dma((len(acts), 2, reach)),
            dma((n_swap, n_fs - 1)),
            dma((n_swap, n_fs - 1)),
        ],
        compiler_params=pltpu.CompilerParams(
            collective_id=collective_id, has_side_effects=True
        ),
        cost_estimate=pl.CostEstimate(flops=0, bytes_accessed=16 * moved, transcendentals=0),
        name=f"gather_tokens_{collective_id}",
    )(*acts, *swaps)


def over_rep(part):
    part = part.astype(jnp.bfloat16)
    n_rep = lax.axis_size("rep")
    other = lax.ppermute(part, "rep", [(i, (i + 1) % n_rep) for i in range(n_rep)])
    return part, other


def added(pair):
    return pair[0].astype(jnp.float32) + pair[1].astype(jnp.float32)


def on_device(tokens, norm_gain, w_gate, w_up, w_down, cotangent):
    n_fs, n_tp = lax.axis_size("fs"), lax.axis_size("tp")
    whole_x, whole_dy, full_gate, full_up, full_down = gather_weights(
        n_fs, n_tp, tokens, cotangent, w_gate, w_up, w_down
    )
    width = whole_x.shape[1]
    wide_tokens = whole_x.astype(jnp.float32)
    gain_f = norm_gain.astype(jnp.float32)
    inverse = lax.rsqrt(jnp.mean(wide_tokens * wide_tokens, axis=-1, keepdims=True) + 1e-06)
    normed = (wide_tokens * inverse * gain_f).astype(jnp.bfloat16)
    gate = jnp.dot(normed, full_gate, preferred_element_type=jnp.float32)
    up_proj = jnp.dot(normed, full_up, preferred_element_type=jnp.float32)
    sigma = jax.nn.sigmoid(gate)
    active = gate * sigma
    hidden = (active * up_proj).astype(jnp.bfloat16)
    back = 0.5 * contract_last(whole_dy, full_down)
    d_up = (back * active).astype(jnp.bfloat16)
    d_gate = (back * up_proj * sigma * (1.0 + gate * (1.0 - sigma))).astype(jnp.bfloat16)

    all_hidden, rows_dy = gather_tokens(n_fs, 1, [hidden], [whole_dy])
    down_pair = over_rep(0.5 * contract_first(all_hidden, rows_dy))

    partial_normed = contract_last(d_gate, full_gate) + contract_last(d_up, full_up)
    d_normed = lax.psum_scatter(
        partial_normed.astype(jnp.bfloat16), "tp", scatter_dimension=1, tiled=True
    ).astype(jnp.float32)

    all_gate, rows_normed = gather_tokens(n_fs, 2, [d_gate], [normed])
    gate_pair = over_rep(contract_first(rows_normed, all_gate))
    (all_up,) = gather_tokens(n_fs, 3, [d_up], [])
    up_pair = over_rep(contract_first(rows_normed, all_up))

    local_width = d_normed.shape[1]
    local_gain = lax.dynamic_slice_in_dim(
        gain_f, lax.axis_index("tp") * local_width, local_width, 0
    )
    local_tokens = tokens.astype(jnp.float32)
    scaled_grad = d_normed * local_gain
    rowdot = lax.psum(jnp.sum(scaled_grad * local_tokens, axis=-1), "tp")
    grad_tokens = (
        cotangent.astype(jnp.float32)
        + inverse * scaled_grad
        - local_tokens * inverse**3 * rowdot[:, None] / width
    ).astype(jnp.bfloat16)
    grad_gain = lax.psum(jnp.sum(d_normed * local_tokens * inverse, axis=0), ("rep", "fs"))

    grad_down = added(down_pair)
    down_sq = lax.psum(jnp.sum(grad_down * grad_down, axis=1), "fs")
    grad_gate = added(gate_pair)
    grad_up = added(up_pair)
    gate_up_sq = lax.psum(
        jnp.stack([jnp.sum(grad_gate * grad_gate, axis=1), jnp.sum(grad_up * grad_up, axis=1)]),
        "tp",
    )
    return (grad_tokens, grad_gain, grad_gate, grad_up, grad_down, gate_up_sq, down_sq)


def solution(mesh):
    placed = (
        P(("rep", "fs"), "tp"),
        P(),
        P("fs", "tp"),
        P("fs", "tp"),
        P("tp", "fs"),
        P(("rep", "fs"), "tp"),
    )
    return jax.shard_map(
        on_device,
        mesh=mesh,
        in_specs=placed,
        out_specs=(
            P(("rep", "fs"), "tp"),
            P("tp"),
            P("fs", "tp"),
            P("fs", "tp"),
            P("tp", "fs"),
            P(None, "fs"),
            P("tp"),
        ),
        check_vma=False,
    )
```

time: 799 us -> 558 us (0.70)
  waiting for transfers between devices: 618 us -> 9.12 us
  Pallas kernels: 0 us -> 441 us
  local copies, waits for them, and re-layouts: 62.5 us -> 2.54 us
  matrix products: 44.9 us -> 33.3 us
    pallas_call x0 -> x4, Pallas kernels: none -> 441 us  [the longest x3 266 us: gather_tokens(): pl.pallas_call(functools.partial(tokens_kernel, n_fs, len(acts), len(swap...]
    all_gather x6 -> x0, waiting for transfers between devices: 347 us -> none  [the longest x1 97.8 us: on_device(): lax.all_gather(w_gate, 'fs', axis=0, tiled=True)]
    reduce_scatter x1 -> x0, waiting for transfers between devices: 238 us -> none  [on_device(): lax.psum_scatter(reordered.astype(jnp.bfloat16), ('rep', 'fs'), scatter_d...]
    convert_element_type x2 -> x0, local copies, waits for them, and re-layouts: 52 us -> none  [on_device(): reordered.astype(jnp.bfloat16)]
    reduce_scatter x1, waiting for transfers between devices: 30.1 us -> 0.02 us  [on_device(): lax.psum_scatter(partial_normed.astype(jnp.bfloat16), 'tp', scatter_dimen...]
    ppermute x0 -> x3, waiting for transfers between devices: none -> 9.08 us  [over_rep(): lax.ppermute(part, 'rep', [(i, (i + 1) % n_rep) for i in range(n_rep)])]
    dot_general x4 -> x5, matrix products: 27 us -> 22.4 us  [the longest x3 16.4 us: contract_first(): lax.dot_general(left, right, (((0,), (0,)), ((), ())), preferred_element_...]
  transfers between devices with their start and end apart: 8 -> 4, of which waited for: 8 -> 1; matrix products, arithmetic and copies ran while one was open for 4% -> 5% of each run, Pallas kernels for 0% -> 48%
where the time goes in v1:
time: 558 us
  Pallas kernels  441 us (79%)
  blocking collectives  37.9 us (7%)
  matrix products  33.3 us (6%)
  other arithmetic  15.9 us (3%)
  between operations  14.3 us (3%)
  waiting for transfers between devices  9.12 us (2%)
    pallas_call x3, Pallas kernels, gather_tokens(): pl.pallas_call(functools.partial(tokens_kernel, n_fs, len(acts), len(swap...  266 us
    pallas_call x1, Pallas kernels, gather_weights(): pl.pallas_call(functools.partial(weights_kernel, n_fs, n_tp), out_shape=[...  175 us
    psum x1, blocking collectives, on_device(): lax.psum(jnp.sum(d_normed * local_tokens * inverse, axis=0), ('rep', 'fs'))  20.1 us
    dot_general x3, matrix products, contract_first(): lax.dot_general(left, right, (((0,), (0,)), ((), ())), preferred_element_...  16.4 us
    psum x1, blocking collectives, on_device(): down_sq = lax.psum(jnp.sum(grad_down * grad_down, axis=1), 'fs')  11.5 us
  transfers between devices with their start and end apart: 4, of which 1 were waited for; matrix products, arithmetic and copies ran while one was open for 5% of the time, Pallas kernels for 48%

profile of v1, /device:TPU:0, one launch (start us, length us, event | category | flops | bytes accessed | tf_op | source)
XLA Modules:
  0.0 557.9 jit_solution(4389122816936145927)
XLA Ops:
  7.2 0.0 reduce-scatter.2.cloned.1.call-start
  7.2 0.7 convert_element_type.62
  7.9 174.9 %gather_weights.1 = (bf16[384,2048]{1,0:T(8,128)(2,1)}, bf16[384,2048]{1,0:T(8,128)(2,1)}, bf16[2048,1280]{1,0:T(8,128)(2,1)}, bf16[2048,1280]{1,0:T(8,128)(2,1)}, bf16[1280,2048]{1,0:T(8,128)(2,1)}) custom-call(bf16[384,512]{1,0:T(8,128)(2,1)} %refs_0_.1, bf16[384,512]{1,0:T(8,128)(2,1)} %refs_1_.1, bf16[512,1280]{1,0:T(8,128)(2,1)} %refs_2_.1, ...), custom_call_target="tpu_custom_call" | custom-call | bytes 301989888 | tf_op jit(solution)/shard_map/gather_weights/pallas_call | solution.py:186
  182.9 1.9 fusion
  184.8 5.3 convolution_multiply_fusion.1
  190.2 0.4 fusion.2.refs_1_
  190.7 2.2 fusion.14
  192.9 0.0 slice-done
  193.0 0.3 slice-done.1
  193.3 3.7 multiply_convert_fusion
  197.0 2.2 fusion.15
  199.2 3.4 add_convert_fusion
  202.6 93.2 %gather_tokens_1.1 = (bf16[1536,1280]{1,0:T(8,128)(2,1)}, bf16[1536,512]{1,0:T(8,128)(2,1)}) custom-call(bf16[384,1280]{1,0:T(8,128)(2,1)} %get-tuple-element.40.refs_0_, bf16[384,2048]{1,0:T(8,128)(2,1)} %get-tuple-element.17.refs_1_), custom_call_target="tpu_custom_call" | custom-call | bytes 88080384 | tf_op jit(solution)/shard_map/gather_tokens_1/pallas_call | solution.py:283
  295.8 5.1 fusion.3
  300.9 1.6 collective-permute-start.2
  302.4 98.4 %gather_tokens_2.1 = (bf16[1536,1280]{1,0:T(8,128)(2,1)}, bf16[1536,512]{1,0:T(8,128)(2,1)}) custom-call(bf16[384,1280]{1,0:T(8,128)(2,1)} %copy-done.6, bf16[384,2048]{1,0:T(8,128)(2,1)} %copy-done), custom_call_target="tpu_custom_call" | custom-call | bytes 88080384 | tf_op jit(solution)/shard_map/gather_tokens_2/pallas_call | solution.py:283
  400.8 5.9 %convolution_convert_fusion.1 = bf16[512,1280]{1,0:T(8,128)(2,1)} fusion(bf16[1536,512]{1,0:T(8,128)(2,1)} %get-tuple-element.21, bf16[1536,1280]{1,0:T(8,128)(2,1)} %get-tuple-element.22), kind=kOutput, calls=%fused_computation.10 | convolution fusion | flops 2013921280 | bytes 6815744 | tf_op jit(solution)/shard_map/dot_general | solution.py:20
  406.7 0.5 collective-permute-start
  407.2 74.8 %gather_tokens_3.1 = bf16[1536,1280]{1,0:T(8,128)(2,1)} custom-call(bf16[384,1280]{1,0:T(8,128)(2,1)} %copy-done.5), custom_call_target="tpu_custom_call" | custom-call | bytes 62914560 | tf_op jit(solution)/shard_map/gather_tokens_3/pallas_call | solution.py:283
  482.0 5.5 convolution_convert_fusion
  487.5 1.5 collective-permute-start.1
  489.0 0.1 dynamic_slice.3
  489.1 2.2 multiply_reduce_fusion
  491.2 2.1 copy.13
  493.3 11.5 %psum.31 = f32[1280]{0:T(1024)} all-reduce(f32[1280]{0:T(1024)S(1)} %get-tuple-element.43), channel_id=1, replica_groups=mesh['rep'=2,'fs'=4,'tp'=4] {'fs'}, use_global_device_ids=true, to_apply=%region_10.0 | all-reduce | flops 1280 | bytes 10240 | tf_op jit(solution)/shard_map/psum | solution.py:362
  504.9 3.6 multiply_reduce_fusion.2
  508.5 9.1 %collective-permute-done.1 = bf16[512,1280]{1,0:T(8,128)(2,1)} collective-permute-done((bf16[512,1280]{1,0:T(8,128)(2,1)}, bf16[512,1280]{1,0:T(8,128)(2,1)}, u32[]{:S(2)}, u32[]{:S(2)}) %collective-permute-start.1) | collective-permute-done | bytes 1310752 | tf_op jit(solution)/shard_map/ppermute | solution.py:307
  517.6 3.6 multiply_reduce_fusion.1
  521.2 1.4 fusion.13
  522.6 20.1 %psum.29 = f32[512]{0:T(512)} all-reduce(f32[512]{0:T(512)S(1)} %get-tuple-element.32), channel_id=1, replica_groups=mesh['rep'=2,'fs'=4,'tp'=4] {'rep','fs'}, use_global_device_ids=true, to_apply=%region_5.0 | all-reduce | flops 512 | bytes 4096 | tf_op jit(solution)/shard_map/psum | solution.py:359
  542.7 6.3 %all-reduce = (f32[384]{0:T(512)S(1)}, f32[2,512]{1,0:T(2,128)}) all-reduce(f32[384]{0:T(512)S(1)} %get-tuple-element.33, f32[2,512]{1,0:T(2,128)S(1)} %pad_maximum_fusion), channel_id=1, replica_groups=mesh['rep'=2,'fs'=4,'tp'=4] {'tp'}, use_global_device_ids=true, to_apply=%region_3.0 | all-reduce | flops 1408 | bytes 11264 | tf_op jit(solution)/shard_map/psum | solution.py:353
  549.0 2.1 fusion.8
  (32 shorter events, 0.1 us)
Async XLA Ops:
  7.2 514.0 %reduce-scatter.2.cloned.1.call-start = ((), (), s32[]{:S(2)}) async-start(), calls=%async_computation.1 | async-start | bytes 1966080 | tf_op jit(solution)/shard_map/reduce_scatter | solution.py:338
  182.9 7.8 %slice-start.2 = ((s8[5242880]{0:T(1024)(128)(4,1)}), s8[4194304]{0:T(1024)(128)(4,1)S(1)}, s32[]{:S(2)}) async-start(s8[5242880]{0:T(1024)(128)(4,1)} %bitcast.22), calls=%async_computation.4 | async-start | bytes 8388608
  184.8 5.4 copy-start.1
  184.8 5.8 %slice-start.3 = ((s8[5242880]{0:T(1024)(128)(4,1)}), s8[1048576]{0:T(1024)(128)(4,1)S(1)}, s32[]{:S(2)}) async-start(s8[5242880]{0:T(1024)(128)(4,1)} %bitcast.22), calls=%async_computation.5 | async-start | bytes 2097152
  190.2 2.8 slice-start
  190.6 2.3 copy-start
  190.7 2.6 slice-start.1
  197.0 2.2 copy-start.6
  197.0 2.2 copy-start.5
  300.9 105.8 %copy-start.4 = (bf16[1280,512]{0,1:T(8,128)(2,1)}, bf16[1280,512]{0,1:T(8,128)(2,1)S(1)}, u32[]{:S(2)}) copy-start(bf16[1280,512]{0,1:T(8,128)(2,1)S(1)} %fusion.3) | copy-start | bytes 3932164
  300.9 188.2 %collective-permute-start.2 = (bf16[1280,512]{0,1:T(8,128)(2,1)S(1)}, bf16[1280,512]{0,1:T(8,128)(2,1)}, u32[]{:S(2)}, u32[]{:S(2)}) collective-permute-start(bf16[1280,512]{0,1:T(8,128)(2,1)S(1)} %fusion.3), channel_id=1, source_target_pairs={{0,16},{16,0},{1,17},{17,1},{2,18},{18,2},{3,19},{19,3},{4,20},{20... | collective-permute-start | bytes 3932168 | tf_op jit(solution)/shard_map/ppermute | solution.py:307
  406.7 75.3 %copy-start.8 = (bf16[1536,512]{1,0:T(8,128)(2,1)S(1)}, bf16[1536,512]{1,0:T(8,128)(2,1)}, u32[]{:S(2)}) copy-start(bf16[1536,512]{1,0:T(8,128)(2,1)} %get-tuple-element.21) | copy-start | bytes 4718596
  406.7 98.2 %collective-permute-start = (bf16[512,1280]{1,0:T(8,128)(2,1)}, bf16[512,1280]{1,0:T(8,128)(2,1)}, u32[]{:S(2)}, u32[]{:S(2)}) collective-permute-start(bf16[512,1280]{1,0:T(8,128)(2,1)} %convolution_convert_fusion.1), channel_id=1, source_target_pairs={{0,16},{16,0},{1,17},{17,1},{2,18},{18,2},{3,19},{19,3},{4,20},{20... | collective-permute-start | bytes 3932168 | tf_op jit(solution)/shard_map/ppermute | solution.py:307
  482.0 7.0 %copy-start.7 = (bf16[2048]{0:T(1024)(128)(2,1)S(1)}, bf16[2048]{0:T(1024)(128)(2,1)}, u32[]{:S(2)}) copy-start(bf16[2048]{0:T(1024)(128)(2,1)} %param.7) | copy-start | bytes 12292
  487.5 30.1 %collective-permute-start.1 = (bf16[512,1280]{1,0:T(8,128)(2,1)}, bf16[512,1280]{1,0:T(8,128)(2,1)}, u32[]{:S(2)}, u32[]{:S(2)}) collective-permute-start(bf16[512,1280]{1,0:T(8,128)(2,1)} %convolution_convert_fusion), channel_id=1, source_target_pairs={{0,16},{16,0},{1,17},{17,1},{2,18},{18,2},{3,19},{19,3},{4,20},{20... | collective-permute-start | bytes 3932168 | tf_op jit(solution)/shard_map/ppermute | solution.py:307
  508.5 12.7 %copy-start.2 = (bf16[384,512]{1,0:T(8,128)(2,1)S(1)}, bf16[384,512]{1,0:T(8,128)(2,1)}, u32[]{:S(2)}) copy-start(bf16[384,512]{1,0:T(8,128)(2,1)} %refs_0_.1) | copy-start | bytes 1179652
  508.5 40.5 %copy-start.3 = (bf16[384,512]{1,0:T(8,128)(2,1)S(1)}, bf16[384,512]{1,0:T(8,128)(2,1)}, u32[]{:S(2)}) copy-start(bf16[384,512]{1,0:T(8,128)(2,1)} %refs_1_.1) | copy-start | bytes 1179652
Sparse Core Ops, SparseCore 0:
  202.8 29.6 reduce-scatter.1

commit v2 on v1

--- a/solution.py
+++ b/solution.py
@@ -22,8 +22,8 @@
     )
 
 
-def send(source, target, send_sem, recv_sem, where):
-    copy = pltpu.make_async_remote_copy(
+def remote(source, target, send_sem, recv_sem, where):
+    return pltpu.make_async_remote_copy(
         src_ref=source,
         dst_ref=target,
         send_sem=send_sem,
@@ -31,8 +31,16 @@
         device_id=where,
         device_id_type=MESH,
     )
-    copy.start()
-    return copy
+
+
+def line_sends(z, n_fs, side, d):
+    if side == 0:
+        return jnp.logical_and(z >= d - 1, z <= n_fs - 2)
+    return jnp.logical_and(z + d <= n_fs, z >= 1)
+
+
+def line_receives(z, n_fs, side, d):
+    return z >= d if side == 0 else z + d <= n_fs - 1
 
 
 def greet(peers):
@@ -76,7 +84,6 @@
     rows = w_gate.shape[0]
     hidden = w_down.shape[0]
     local = tokens.shape[1]
-    reach = n_fs // 2
 
     def own_piece(m, half):
         size = (hidden if m == 2 else rows) // 2
@@ -98,36 +105,55 @@
     peers += [{"tp": lax.rem(t + j, n_tp)} for j in range(1, n_tp)]
     greet(peers)
 
-    ends = []
+    def owner_of(side, back):
+        return lax.rem(z + (n_fs - back if side == 0 else back), n_fs)
 
     def hop(m, side, d):
-        half = r if side == 0 else 1 - r
-        owner = lax.rem(z + (n_fs - (d - 1) if side == 0 else d - 1), n_fs)
-        place = piece(m, owner, half)
-        return send(
-            own_piece(m, half) if d == 1 else place,
+        place = piece(m, owner_of(side, d - 1), r)
+        return remote(
+            own_piece(m, r) if d == 1 else place,
             place,
             ring_send.at[m, side, d - 1],
             ring_recv.at[m, side, d - 1],
             {"fs": right if side == 0 else left},
         )
 
-    flying = {}
+    def arrival(m, side, d):
+        place = piece(m, owner_of(side, d), r)
+        return remote(
+            place,
+            place,
+            ring_send.at[m, side, d - 1],
+            ring_recv.at[m, side, d - 1],
+            {"fs": right if side == 0 else left},
+        )
+
+    def across(m, side, d):
+        place = piece(m, owner_of(side, d), r)
+        return remote(
+            place, place, rep_send.at[m, side, d - 1], rep_recv.at[m, side, d - 1], partner
+        )
+
     for m in range(3):
         for side in range(2):
-            flying[m, side] = hop(m, side, 1)
+
+            @pl.when(line_sends(z, n_fs, side, 1))
+            def _():
+                hop(m, side, 1).start()
+
+    ends = []
     for a, (source, target) in enumerate(((tokens, whole_x), (cot, whole_dy))):
         place = target.at[:, pl.ds(pl.multiple_of(t * local, local), local)]
         for j in range(1, n_tp):
-            ends.append(
-                send(
-                    source,
-                    place,
-                    tp_send.at[a, j - 1],
-                    tp_recv.at[a, j - 1],
-                    {"tp": lax.rem(t + j, n_tp)},
-                )
+            copy = remote(
+                source,
+                place,
+                tp_send.at[a, j - 1],
+                tp_recv.at[a, j - 1],
+                {"tp": lax.rem(t + j, n_tp)},
             )
+            copy.start()
+            ends.append(copy)
     mine = pl.ds(pl.multiple_of(t * local, local), local)
     band = pl.ds(pl.multiple_of(z * rows, rows), rows)
     finish = keep_own(
@@ -143,26 +169,33 @@
         own_sem,
     )
     finish()
-    for d in range(1, reach + 1):
+    for d in range(1, n_fs):
         for m in range(3):
             for side in range(2):
-                copy = flying[m, side]
-                copy.wait_recv()
-                if d < reach:
-                    flying[m, side] = hop(m, side, d + 1)
-                    half = r if side == 0 else 1 - r
-                    owner = lax.rem(z + (n_fs - d if side == 0 else d), n_fs)
-                    place = piece(m, owner, half)
-                    ends.append(
-                        send(
-                            place,
-                            place,
-                            rep_send.at[m, side, d - 1],
-                            rep_recv.at[m, side, d - 1],
-                            partner,
-                        )
-                    )
-                copy.wait_send()
+
+                @pl.when(line_receives(z, n_fs, side, d))
+                def _():
+                    arrival(m, side, d).wait_recv()
+                    if d < n_fs - 1:
+
+                        @pl.when(line_sends(z, n_fs, side, d + 1))
+                        def _():
+                            hop(m, side, d + 1).start()
+
+                    across(m, side, d).start()
+
+    for d in range(1, n_fs):
+        for m in range(3):
+            for side in range(2):
+
+                @pl.when(line_sends(z, n_fs, side, d))
+                def _():
+                    hop(m, side, d).wait_send()
+
+                @pl.when(line_receives(z, n_fs, side, d))
+                def _():
+                    across(m, side, d).wait()
+
     for copy in ends:
         copy.wait()
 
@@ -180,7 +213,6 @@
         (hidden, width),
     ]
     held = (tokens, cot, w_gate, w_up, w_down)
-    reach = n_fs // 2
     moved = sum(2 * a * b for a, b in shapes)
     dma = pltpu.SemaphoreType.DMA
     return pl.pallas_call(
@@ -191,10 +223,10 @@
         scratch_shapes=[pltpu.VMEM(a.shape, a.dtype) for a in held]
         + [
             dma((2, 5)),
-            dma((3, 2, reach)),
-            dma((3, 2, reach)),
-            dma((3, 2, max(reach - 1, 1))),
-            dma((3, 2, max(reach - 1, 1))),
+            dma((3, 2, n_fs - 1)),
+            dma((3, 2, n_fs - 1)),
+            dma((3, 2, n_fs - 1)),
+            dma((3, 2, n_fs - 1)),
             dma((2, n_tp - 1)),
             dma((2, n_tp - 1)),
         ],
@@ -204,93 +236,174 @@
     )(*held)
 
 
-def tokens_kernel(n_fs, n_act, n_swap, *refs):
+def tokens_kernel(n_fs, n_tp, n_act, n_swap, *refs):
     total = n_act + n_swap
     acts, swaps = refs[:n_act], refs[n_act:total]
     act_outs, swap_outs = refs[total : total + n_act], refs[total + n_act : 2 * total]
     holders = refs[2 * total : 3 * total]
-    own_sem, ring_send, ring_recv, swap_send, swap_recv = refs[3 * total :]
-    z = lax.axis_index("fs")
+    own_sem, ring_send, ring_recv = refs[3 * total : 3 * total + 3]
+    swap_send, swap_recv, relay_send, relay_recv = refs[3 * total + 3 :]
+    z, t = lax.axis_index("fs"), lax.axis_index("tp")
     right, left = lax.rem(z + 1, n_fs), lax.rem(z + n_fs - 1, n_fs)
     count = acts[0].shape[0]
-    reach = n_fs // 2
-    greet([{"fs": lax.rem(z + j, n_fs)} for j in range(1, n_fs)])
+    peers = [{"fs": lax.rem(z + j, n_fs)} for j in range(1, n_fs)]
+    if n_swap:
+        peers += [{"tp": lax.rem(t + j, n_tp)} for j in range(1, n_tp)]
+    greet(peers)
+
+    def rows_of(owner):
+        return pl.ds(pl.multiple_of(owner * count, count), count)
+
+    def owner_of(side, back):
+        return lax.rem(z + (n_fs - back if side == 0 else back), n_fs)
 
     def hop(m, side, d):
-        owner = lax.rem(z + (n_fs - (d - 1) if side == 0 else d - 1), n_fs)
-        first, size = 0, count
-        if d == reach:
-            size = count // 2
-            first = side * size
-        place = act_outs[m].at[pl.ds(pl.multiple_of(owner * count + first, size), size), :]
-        source = acts[m].at[pl.ds(first, size), :] if d == 1 else place
-        return send(
-            source,
+        place = act_outs[m].at[rows_of(owner_of(side, d - 1)), :]
+        return remote(
+            acts[m] if d == 1 else place,
             place,
             ring_send.at[m, side, d - 1],
             ring_recv.at[m, side, d - 1],
             {"fs": right if side == 0 else left},
         )
 
-    ends = []
-    flying = {}
-    band = pl.ds(pl.multiple_of(z * count, count), count)
+    def arrival(m, side, d):
+        place = act_outs[m].at[rows_of(owner_of(side, d)), :]
+        return remote(
+            place,
+            place,
+            ring_send.at[m, side, d - 1],
+            ring_recv.at[m, side, d - 1],
+            {"fs": right if side == 0 else left},
+        )
+
+    def swap(a, j):
+        peer = lax.rem(z + j, n_fs)
+        cut = swap_outs[a].shape[1]
+        return remote(
+            swaps[a].at[:, pl.ds(pl.multiple_of(peer * cut, cut), cut)],
+            swap_outs[a].at[rows_of(z), :],
+            swap_send.at[a, j - 1],
+            swap_recv.at[a, j - 1],
+            {"fs": peer},
+        )
+
+    def swapped(a, j):
+        place = swap_outs[a].at[rows_of(owner_of(0, j)), :]
+        return remote(
+            place,
+            place,
+            swap_send.at[a, j - 1],
+            swap_recv.at[a, j - 1],
+            {"fs": lax.rem(z + j, n_fs)},
+        )
+
+    def relay(a, j, k):
+        place = swap_outs[a].at[rows_of(owner_of(0, j)), :]
+        return remote(
+            place,
+            place,
+            relay_send.at[a, j - 1, k - 1],
+            relay_recv.at[a, j - 1],
+            {"tp": lax.rem(t + k, n_tp)},
+        )
+
+    hub = lax.rem(z, n_tp) == t
+
+    def feeds(j):
+        return lax.rem(lax.rem(z + j, n_fs), n_tp) == t
+
+    for a in range(n_swap):
+        for j in range(1, n_fs):
+
+            @pl.when(feeds(j))
+            def _():
+                swap(a, j).start()
+
     for m in range(n_act):
         for side in range(2):
-            flying[m, side] = hop(m, side, 1)
-    for a in range(n_swap):
-        cut = swap_outs[a].shape[1]
-        for j in range(1, n_fs):
-            peer = lax.rem(z + j, n_fs)
-            ends.append(
-                send(
-                    swaps[a].at[:, pl.ds(pl.multiple_of(peer * cut, cut), cut)],
-                    swap_outs[a].at[band, :],
-                    swap_send.at[a, j - 1],
-                    swap_recv.at[a, j - 1],
-                    {"fs": peer},
-                )
-            )
+
+            @pl.when(line_sends(z, n_fs, side, 1))
+            def _():
+                hop(m, side, 1).start()
+
     sources = list(acts)
     for a in range(n_swap):
         cut = swap_outs[a].shape[1]
         sources.append(swaps[a].at[:, pl.ds(pl.multiple_of(z * cut, cut), cut)])
     finish = keep_own(
-        sources, holders, [out.at[band, :] for out in act_outs + swap_outs], own_sem
+        sources, holders, [out.at[rows_of(z), :] for out in act_outs + swap_outs], own_sem
     )
     finish()
-    for d in range(1, reach + 1):
+    if n_swap:
+
+        @pl.when(hub)
+        def _():
+            for a in range(n_swap):
+                for j in range(1, n_fs):
+                    swapped(a, j).wait_recv()
+                    for k in range(1, n_tp):
+                        relay(a, j, k).start()
+
+    for d in range(1, n_fs):
         for m in range(n_act):
             for side in range(2):
-                copy = flying[m, side]
-                copy.wait_recv()
-                if d < reach:
-                    flying[m, side] = hop(m, side, d + 1)
-                copy.wait_send()
-    for copy in ends:
-        copy.wait()
-
-
-def gather_tokens(n_fs, collective_id, acts, swaps):
+
+                @pl.when(line_receives(z, n_fs, side, d))
+                def _():
+                    arrival(m, side, d).wait_recv()
+                    if d < n_fs - 1:
+
+                        @pl.when(line_sends(z, n_fs, side, d + 1))
+                        def _():
+                            hop(m, side, d + 1).start()
+
+    for d in range(1, n_fs):
+        for m in range(n_act):
+            for side in range(2):
+
+                @pl.when(line_sends(z, n_fs, side, d))
+                def _():
+                    hop(m, side, d).wait_send()
+
+    for a in range(n_swap):
+        for j in range(1, n_fs):
+
+            @pl.when(feeds(j))
+            def _():
+                swap(a, j).wait_send()
+
+            @pl.when(hub)
+            def _():
+                for k in range(1, n_tp):
+                    relay(a, j, k).wait_send()
+
+            @pl.when(jnp.logical_not(hub))
+            def _():
+                relay(a, j, 1).wait_recv()
+
+
+def gather_tokens(n_fs, n_tp, collective_id, acts, swaps):
     count = acts[0].shape[0]
     outs = [jax.ShapeDtypeStruct((n_fs * count, a.shape[1]), a.dtype) for a in acts]
     outs += [jax.ShapeDtypeStruct((n_fs * count, a.shape[1] // n_fs), a.dtype) for a in swaps]
-    reach = n_fs // 2
     dma = pltpu.SemaphoreType.DMA
     total = len(outs)
     n_swap = max(len(swaps), 1)
     moved = sum(2 * o.shape[0] * o.shape[1] for o in outs)
     return pl.pallas_call(
-        functools.partial(tokens_kernel, n_fs, len(acts), len(swaps)),
+        functools.partial(tokens_kernel, n_fs, n_tp, len(acts), len(swaps)),
         out_shape=outs,
         in_specs=[pl.BlockSpec(memory_space=pl.ANY)] * total,
         out_specs=[pl.BlockSpec(memory_space=pl.ANY)] * total,
         scratch_shapes=[pltpu.VMEM((count, o.shape[1]), o.dtype) for o in outs]
         + [
             dma((2, total)),
-            dma((len(acts), 2, reach)),
-            dma((len(acts), 2, reach)),
+            dma((len(acts), 2, n_fs - 1)),
+            dma((len(acts), 2, n_fs - 1)),
             dma((n_swap, n_fs - 1)),
+            dma((n_swap, n_fs - 1)),
+            dma((n_swap, n_fs - 1, n_tp - 1)),
             dma((n_swap, n_fs - 1)),
         ],
         compiler_params=pltpu.CompilerParams(
@@ -331,7 +444,7 @@
     d_up = (back * active).astype(jnp.bfloat16)
     d_gate = (back * up_proj * sigma * (1.0 + gate * (1.0 - sigma))).astype(jnp.bfloat16)
 
-    all_hidden, rows_dy = gather_tokens(n_fs, 1, [hidden], [whole_dy])
+    all_hidden, rows_dy = gather_tokens(n_fs, n_tp, 1, [hidden], [whole_dy])
     down_pair = over_rep(0.5 * contract_first(all_hidden, rows_dy))
 
     partial_normed = contract_last(d_gate, full_gate) + contract_last(d_up, full_up)
@@ -339,9 +452,9 @@
         partial_normed.astype(jnp.bfloat16), "tp", scatter_dimension=1, tiled=True
     ).astype(jnp.float32)
 
-    all_gate, rows_normed = gather_tokens(n_fs, 2, [d_gate], [normed])
+    all_gate, rows_normed = gather_tokens(n_fs, n_tp, 2, [d_gate], [normed])
     gate_pair = over_rep(contract_first(rows_normed, all_gate))
-    (all_up,) = gather_tokens(n_fs, 3, [d_up], [])
+    (all_up,) = gather_tokens(n_fs, n_tp, 3, [d_up], [])
     up_pair = over_rep(contract_first(rows_normed, all_up))
 
     local_width = d_normed.shape[1]

time: 558 us -> 501 us (0.90)
  Pallas kernels: 441 us -> 385 us
    pallas_call x3, Pallas kernels: 266 us -> 236 us  [gather_tokens(): pl.pallas_call(functools.partial(tokens_kernel, n_fs, n_tp, len(acts), le...]
    pallas_call x1, Pallas kernels: 175 us -> 149 us  [gather_weights(): pl.pallas_call(functools.partial(weights_kernel, n_fs, n_tp), out_shape=[...]
  transfers between devices with their start and end apart: 4 -> 4, of which waited for: 1 -> 1; matrix products, arithmetic and copies ran while one was open for 5% -> 6% of each run, Pallas kernels for 48% -> 47%
where the time goes in v2:
time: 501 us; the launch traced here: 500 us
  Pallas kernels  385 us (77%)
  blocking collectives  37.8 us (8%)
  matrix products  33.1 us (7%)
  other arithmetic  15.9 us (3%)
  between operations  14.3 us (3%)
  waiting for transfers between devices  8.43 us (2%)
    pallas_call x3, Pallas kernels, gather_tokens(): pl.pallas_call(functools.partial(tokens_kernel, n_fs, n_tp, len(acts), le...  236 us
    pallas_call x1, Pallas kernels, gather_weights(): pl.pallas_call(functools.partial(weights_kernel, n_fs, n_tp), out_shape=[...  149 us
    psum x1, blocking collectives, on_device(): lax.psum(jnp.sum(d_normed * local_tokens * inverse, axis=0), ('rep', 'fs'))  20.5 us
    dot_general x3, matrix products, contract_first(): lax.dot_general(left, right, (((0,), (0,)), ((), ())), preferred_element_...  16.2 us
    psum x1, blocking collectives, on_device(): down_sq = lax.psum(jnp.sum(grad_down * grad_down, axis=1), 'fs')  10.9 us
    dot_general x3, matrix products, contract_last(): lax.dot_general(left, right, (((1,), (1,)), ((), ())), preferred_element_...  10.9 us
  transfers between devices with their start and end apart: 4, of which 1 were waited for; matrix products, arithmetic and copies ran while one was open for 6% of the time, Pallas kernels for 47%

profile of v2, /device:TPU:0, one launch (start us, length us, event | category | flops | bytes accessed | tf_op | source)
XLA Modules:
  0.0 500.0 jit_solution(8675198434028722563)
XLA Ops:
  7.2 0.0 reduce-scatter.2.cloned.1.call-start
  7.2 0.7 convert_element_type.62
  7.9 149.3 %gather_weights.1 = (bf16[384,2048]{1,0:T(8,128)(2,1)}, bf16[384,2048]{1,0:T(8,128)(2,1)}, bf16[2048,1280]{1,0:T(8,128)(2,1)}, bf16[2048,1280]{1,0:T(8,128)(2,1)}, bf16[1280,2048]{1,0:T(8,128)(2,1)}) custom-call(bf16[384,512]{1,0:T(8,128)(2,1)} %refs_0_.1, bf16[384,512]{1,0:T(8,128)(2,1)} %refs_1_.1, bf16[512,1280]{1,0:T(8,128)(2,1)} %refs_2_.1, ...), custom_call_target="tpu_custom_call" | custom-call | bytes 301989888 | tf_op jit(solution)/shard_map/gather_weights/pallas_call | solution.py:218
  157.2 1.9 fusion
  159.2 5.3 %convolution_multiply_fusion.1 = f32[384,1280]{1,0:T(8,128)S(1)} fusion(bf16[384,2048]{1,0:T(8,128)(2,1)} %get-tuple-element.17.refs_1_, bf16[1280,2048]{1,0:T(8,128)(2,1)} %get-tuple-element.18), kind=kOutput, calls=%fused_computation.7 | convolution fusion | flops 2013757440 | bytes 8781824 | tf_op jit(solution)/shard_map/dot_general | solution.py:14
  164.6 0.4 fusion.2.refs_1_
  165.1 2.2 fusion.14
  167.3 0.0 slice-done
  167.3 0.3 slice-done.1
  167.6 3.7 multiply_convert_fusion
  171.4 2.2 fusion.15
  173.6 3.4 add_convert_fusion
  177.0 84.5 %gather_tokens_1.1 = (bf16[1536,1280]{1,0:T(8,128)(2,1)}, bf16[1536,512]{1,0:T(8,128)(2,1)}) custom-call(bf16[384,1280]{1,0:T(8,128)(2,1)} %get-tuple-element.40.refs_0_, bf16[384,2048]{1,0:T(8,128)(2,1)} %get-tuple-element.17.refs_1_), custom_call_target="tpu_custom_call" | custom-call | bytes 88080384 | tf_op jit(solution)/shard_map/gather_tokens_1/pallas_call | solution.py:394
  261.5 4.8 fusion.3
  266.4 0.6 collective-permute-start.2
  267.0 85.9 %gather_tokens_2.1 = (bf16[1536,1280]{1,0:T(8,128)(2,1)}, bf16[1536,512]{1,0:T(8,128)(2,1)}) custom-call(bf16[384,1280]{1,0:T(8,128)(2,1)} %copy-done.6, bf16[384,2048]{1,0:T(8,128)(2,1)} %copy-done), custom_call_target="tpu_custom_call" | custom-call | bytes 88080384 | tf_op jit(solution)/shard_map/gather_tokens_2/pallas_call | solution.py:394
  352.9 5.9 %convolution_convert_fusion.1 = bf16[512,1280]{1,0:T(8,128)(2,1)} fusion(bf16[1536,512]{1,0:T(8,128)(2,1)} %get-tuple-element.21, bf16[1536,1280]{1,0:T(8,128)(2,1)} %get-tuple-element.22), kind=kOutput, calls=%fused_computation.10 | convolution fusion | flops 2013921280 | bytes 6815744 | tf_op jit(solution)/shard_map/dot_general | solution.py:20
  358.8 1.5 collective-permute-start
  360.3 65.5 %gather_tokens_3.1 = bf16[1536,1280]{1,0:T(8,128)(2,1)} custom-call(bf16[384,1280]{1,0:T(8,128)(2,1)} %copy-done.5), custom_call_target="tpu_custom_call" | custom-call | bytes 62914560 | tf_op jit(solution)/shard_map/gather_tokens_3/pallas_call | solution.py:394
  425.9 5.5 %convolution_convert_fusion = bf16[512,1280]{1,0:T(8,128)(2,1)} fusion(bf16[1536,512]{1,0:T(8,128)(2,1)S(1)} %copy-done.8, bf16[1536,1280]{1,0:T(8,128)(2,1)} %gather_tokens_3.1), kind=kOutput, calls=%fused_computation.9 | convolution fusion | flops 2013921280 | bytes 6815744 | tf_op jit(solution)/shard_map/dot_general | solution.py:20
  431.4 0.5 collective-permute-start.1
  431.9 0.1 dynamic_slice.3
  432.0 2.2 multiply_reduce_fusion
  434.1 2.1 copy.13
  436.2 10.9 %psum.31 = f32[1280]{0:T(1024)} all-reduce(f32[1280]{0:T(1024)S(1)} %get-tuple-element.43), channel_id=1, replica_groups=mesh['rep'=2,'fs'=4,'tp'=4] {'fs'}, use_global_device_ids=true, to_apply=%region_10.0 | all-reduce | flops 1280 | bytes 10240 | tf_op jit(solution)/shard_map/psum | solution.py:475
  447.2 3.6 multiply_reduce_fusion.2
  450.8 8.4 %collective-permute-done.1 = bf16[512,1280]{1,0:T(8,128)(2,1)} collective-permute-done((bf16[512,1280]{1,0:T(8,128)(2,1)}, bf16[512,1280]{1,0:T(8,128)(2,1)}, u32[]{:S(2)}, u32[]{:S(2)}) %collective-permute-start.1) | collective-permute-done | bytes 1310752 | tf_op jit(solution)/shard_map/ppermute | solution.py:420
  459.2 3.6 multiply_reduce_fusion.1
  462.9 1.4 fusion.13
  464.2 20.5 %psum.29 = f32[512]{0:T(512)} all-reduce(f32[512]{0:T(512)S(1)} %get-tuple-element.32), channel_id=1, replica_groups=mesh['rep'=2,'fs'=4,'tp'=4] {'rep','fs'}, use_global_device_ids=true, to_apply=%region_5.0 | all-reduce | flops 512 | bytes 4096 | tf_op jit(solution)/shard_map/psum | solution.py:472
  484.7 6.4 %all-reduce = (f32[384]{0:T(512)S(1)}, f32[2,512]{1,0:T(2,128)}) all-reduce(f32[384]{0:T(512)S(1)} %get-tuple-element.33, f32[2,512]{1,0:T(2,128)S(1)} %pad_maximum_fusion), channel_id=1, replica_groups=mesh['rep'=2,'fs'=4,'tp'=4] {'tp'}, use_global_device_ids=true, to_apply=%region_3.0 | all-reduce | flops 1408 | bytes 11264 | tf_op jit(solution)/shard_map/psum | solution.py:466
  491.1 2.1 fusion.8
  (32 shorter events, 0.1 us)
Async XLA Ops:
  7.2 455.7 %reduce-scatter.2.cloned.1.call-start = ((), (), s32[]{:S(2)}) async-start(), calls=%async_computation.1 | async-start | bytes 1966080 | tf_op jit(solution)/shard_map/reduce_scatter | solution.py:451
  157.2 7.8 %slice-start.2 = ((s8[5242880]{0:T(1024)(128)(4,1)}), s8[4194304]{0:T(1024)(128)(4,1)S(1)}, s32[]{:S(2)}) async-start(s8[5242880]{0:T(1024)(128)(4,1)} %bitcast.22), calls=%async_computation.4 | async-start | bytes 8388608
  159.2 5.4 %copy-start.1 = (bf16[384,2048]{1,0:T(8,128)(2,1)S(1)}, bf16[384,2048]{1,0:T(8,128)(2,1)}, u32[]{:S(2)}) copy-start(bf16[384,2048]{1,0:T(8,128)(2,1)} %get-tuple-element.16) | copy-start | bytes 4718596
  159.2 5.8 %slice-start.3 = ((s8[5242880]{0:T(1024)(128)(4,1)}), s8[1048576]{0:T(1024)(128)(4,1)S(1)}, s32[]{:S(2)}) async-start(s8[5242880]{0:T(1024)(128)(4,1)} %bitcast.22), calls=%async_computation.5 | async-start | bytes 2097152
  164.6 2.8 slice-start
  165.0 2.3 copy-start
  165.1 2.6 slice-start.1
  171.4 2.2 copy-start.6
  171.4 2.2 copy-start.5
  266.4 92.5 %copy-start.4 = (bf16[1280,512]{0,1:T(8,128)(2,1)}, bf16[1280,512]{0,1:T(8,128)(2,1)S(1)}, u32[]{:S(2)}) copy-start(bf16[1280,512]{0,1:T(8,128)(2,1)S(1)} %fusion.3) | copy-start | bytes 3932164
  266.4 165.6 %collective-permute-start.2 = (bf16[1280,512]{0,1:T(8,128)(2,1)S(1)}, bf16[1280,512]{0,1:T(8,128)(2,1)}, u32[]{:S(2)}, u32[]{:S(2)}) collective-permute-start(bf16[1280,512]{0,1:T(8,128)(2,1)S(1)} %fusion.3), channel_id=1, source_target_pairs={{0,16},{16,0},{1,17},{17,1},{2,18},{18,2},{3,19},{19,3},{4,20},{20... | collective-permute-start | bytes 3932168 | tf_op jit(solution)/shard_map/ppermute | solution.py:420
  358.8 67.0 %copy-start.8 = (bf16[1536,512]{1,0:T(8,128)(2,1)S(1)}, bf16[1536,512]{1,0:T(8,128)(2,1)}, u32[]{:S(2)}) copy-start(bf16[1536,512]{1,0:T(8,128)(2,1)} %get-tuple-element.21) | copy-start | bytes 4718596
  358.8 88.4 %collective-permute-start = (bf16[512,1280]{1,0:T(8,128)(2,1)}, bf16[512,1280]{1,0:T(8,128)(2,1)}, u32[]{:S(2)}, u32[]{:S(2)}) collective-permute-start(bf16[512,1280]{1,0:T(8,128)(2,1)} %convolution_convert_fusion.1), channel_id=1, source_target_pairs={{0,16},{16,0},{1,17},{17,1},{2,18},{18,2},{3,19},{19,3},{4,20},{20... | collective-permute-start | bytes 3932168 | tf_op jit(solution)/shard_map/ppermute | solution.py:420
  425.9 6.0 %copy-start.7 = (bf16[2048]{0:T(1024)(128)(2,1)S(1)}, bf16[2048]{0:T(1024)(128)(2,1)}, u32[]{:S(2)}) copy-start(bf16[2048]{0:T(1024)(128)(2,1)} %param.7) | copy-start | bytes 12292
  431.4 27.8 %collective-permute-start.1 = (bf16[512,1280]{1,0:T(8,128)(2,1)}, bf16[512,1280]{1,0:T(8,128)(2,1)}, u32[]{:S(2)}, u32[]{:S(2)}) collective-permute-start(bf16[512,1280]{1,0:T(8,128)(2,1)} %convolution_convert_fusion), channel_id=1, source_target_pairs={{0,16},{16,0},{1,17},{17,1},{2,18},{18,2},{3,19},{19,3},{4,20},{20... | collective-permute-start | bytes 3932168 | tf_op jit(solution)/shard_map/ppermute | solution.py:420
  450.8 12.1 %copy-start.2 = (bf16[384,512]{1,0:T(8,128)(2,1)S(1)}, bf16[384,512]{1,0:T(8,128)(2,1)}, u32[]{:S(2)}) copy-start(bf16[384,512]{1,0:T(8,128)(2,1)} %refs_0_.1) | copy-start | bytes 1179652
  450.8 40.3 %copy-start.3 = (bf16[384,512]{1,0:T(8,128)(2,1)S(1)}, bf16[384,512]{1,0:T(8,128)(2,1)}, u32[]{:S(2)}) copy-start(bf16[384,512]{1,0:T(8,128)(2,1)} %refs_1_.1) | copy-start | bytes 1179652
Sparse Core Ops, SparseCore 0:
  177.1 27.0 reduce-scatter.1
